TPU v7x, 32 devices: a whole 2x2x4 slice. The times are simulated.
32 devices in a mesh: kv: 8 (over y, x, core), tp: 4 (over z).
Axes of the slice: x: 2, y: 2, z: 4, core: 2. Of those that a mesh axis runs over, the one named last changes fastest.
Arguments:
- tokens: bfloat16 [320, 4096], P('tp', 'kv'), may hold values from -8 to 8
- state: float32 [320, 32, 128, 128], P('kv', 'tp'), may hold values from -4 to 4
- mix_gain: float32 [4096], P('kv'), may hold values from 0.1 to 1.9
- q_weight: bfloat16 [4096, 4096], P('kv', 'tp'), may hold values from -0.09375 to 0.09375
- forget_weight: bfloat16 [4096, 4096], P('kv', 'tp'), may hold values from -0.09375 to 0.09375
- input_weight: bfloat16 [4096, 4096], P('kv', 'tp'), may hold values from -0.09375 to 0.09375
- gate_weight: bfloat16 [4096, 4096], P('kv', 'tp'), may hold values from -0.09375 to 0.09375
- lower_bound: float32 [4096], P('tp'), may hold values from 0 to 0.9
- head_gain: float32 [128], replicated, may hold values from 0.1 to 1.9
- out_weight: bfloat16 [4096, 4096], P('tp', 'kv'), may hold values from -0.09375 to 0.09375
- ffn_gain: float32 [4096], P('kv'), may hold values from 0.1 to 1.9
- ffn_gate: bfloat16 [4096, 10240], P('kv', 'tp'), may hold values from -0.09375 to 0.09375
- ffn_up: bfloat16 [4096, 10240], P('kv', 'tp'), may hold values from -0.09375 to 0.09375
- ffn_down: bfloat16 [10240, 4096], P('tp', 'kv'), may hold values from -0.0625 to 0.0625
Outputs:
- layer_out: bfloat16 [320, 4096], P('tp', 'kv')
- new_state: float32 [320, 32, 128, 128], P('kv', 'tp')
All inputs are finite; a program needn't handle non-finite values.
Results may differ from a plain program's by a relative error of at most 0.007.
Values may be sent and summed in bfloat16 or wider, within the bound.
A program may use at most 128 MiB of HBM per device.

v0:
```python
import jax
import jax.numpy as jnp
from jax import lax
from jax.sharding import PartitionSpec as P

EPS = 1e-05


def project_in(shard_rows, norm_gain, weight_joined, width):
    rows_all = lax.all_gather(shard_rows, "tp", axis=0, tiled=True)
    values = rows_all.astype(jnp.float32)
    squares = jnp.sum(values * values, axis=1)
    normed = (values * norm_gain).astype(jnp.bfloat16)
    product = jnp.dot(normed, weight_joined, preferred_element_type=jnp.float32)
    sums, totals = (
        lax.psum_scatter(product, "kv", scatter_dimension=0, tiled=True),
        lax.psum_scatter(squares, "kv", scatter_dimension=0, tiled=True),
    )
    sums = sums * lax.rsqrt(totals / width + EPS)[:, None]
    return (rows_all, sums)


def project_back(shard_rows, weight):
    return jnp.dot(
        lax.all_gather(shard_rows, "kv", axis=0, tiled=True),
        weight,
        preferred_element_type=jnp.float32,
    )


def sum_widths(terms):
    return lax.psum_scatter(terms, "tp", scatter_dimension=0, tiled=True)


def body(
    tokens,
    state,
    mix_gain,
    q_weight,
    forget_weight,
    input_weight,
    gate_weight,
    lower_bound,
    head_gain,
    out_weight,
    ffn_gain,
    ffn_gate,
    ffn_up,
    ffn_down,
):
    width = tokens.shape[1] * lax.axis_size("kv")
    mixer_joined = jnp.concatenate((q_weight, forget_weight, input_weight, gate_weight), axis=1)
    ffn_joined = jnp.concatenate((ffn_gate, ffn_up), axis=1)
    whole_tokens, mixer_sums = project_in(tokens, mix_gain, mixer_joined, width)
    head_cols = q_weight.shape[1]
    seq_rows = mixer_sums.shape[0]
    heads_here = state.shape[1]
    head_size = state.shape[2]
    split_shape = (seq_rows, heads_here, head_size)
    query = (jax.nn.silu(mixer_sums[:, :head_cols]) * head_size ** (-0.5)).reshape(split_shape)
    forget = lower_bound + (1.0 - lower_bound) * jax.nn.sigmoid(
        mixer_sums[:, head_cols : 2 * head_cols]
    )
    forget = forget.reshape(split_shape)
    value = mixer_sums[:, 2 * head_cols : 3 * head_cols].reshape(split_shape)
    gate_pre = mixer_sums[:, 3 * head_cols :]
    new_state = forget[..., None] * state + (1.0 - forget)[..., None] * value[:, :, None, :]
    read = jnp.einsum("bhk,bhkv->bhv", query, new_state, precision=lax.Precision.HIGHEST)
    read = read * lax.rsqrt(jnp.mean(read * read, axis=-1, keepdims=True) + EPS) * head_gain
    gated = (read.reshape(seq_rows, head_cols) * jax.nn.silu(gate_pre)).astype(jnp.bfloat16)
    attended_terms = project_back(gated, out_weight)
    attended = sum_widths(attended_terms)
    own_rows = (tokens.astype(jnp.float32) + attended).astype(jnp.bfloat16)
    unused_rows, ffn_sums = project_in(own_rows, ffn_gain, ffn_joined, width)
    ffn_cols = ffn_gate.shape[1]
    hidden = (jax.nn.silu(ffn_sums[:, :ffn_cols]) * ffn_sums[:, ffn_cols:]).astype(jnp.bfloat16)
    layer_out = (own_rows.astype(jnp.float32) + sum_widths(project_back(hidden, ffn_down))).astype(
        jnp.bfloat16
    )
    return (layer_out, new_state)


def solution(mesh):
    in_specs = (
        P("tp", "kv"),
        P("kv", "tp", None, None),
        P("kv"),
        P("kv", "tp"),
        P("kv", "tp"),
        P("kv", "tp"),
        P("kv", "tp"),
        P("tp"),
        P(),
        P("tp", "kv"),
        P("kv"),
        P("kv", "tp"),
        P("kv", "tp"),
        P("tp", "kv"),
    )
    out_specs = (P("tp", "kv"), P("kv", "tp", None, None))
    return jax.shard_map(body, mesh=mesh, in_specs=in_specs, out_specs=out_specs, check_vma=False)
```

profile of v0, /device:TPU:0, one launch (start us, length us, event | category | flops | bytes accessed | tf_op | source)
XLA Modules:
  0.0 304.2 jit_solution(6236995750941943419)
XLA Ops:
  7.2 16.2 %all_gather.12 = bf16[320,512]{1,0:T(8,128)(2,1)S(1)} all-gather(bf16[80,512]{1,0:T(8,128)(2,1)} %param.14), channel_id=1, replica_groups=mesh['kv'=8,'tp'=4] {'tp'}, dimensions={0}, use_global_device_ids=true | all-gather | bytes 409600 | tf_op jit(solution)/shard_map/all_gather | solution.py:10
  23.4 6.1 %fusion.4 = f32[320,4096]{1,0:T(8,128)} fusion(bf16[512,1024]{1,0:T(8,128)(2,1)} %param.20, bf16[512,1024]{1,0:T(8,128)(2,1)} %param.19, bf16[512,1024]{1,0:T(8,128)(2,1)} %param.18, bf16[512,1024]{1,0:T(8,128)(2,1)} %param.17, bf16[320,512]{1,0:T(8,128)(2,1)S(1)} %all_gather.12, f32[512]{0:T(512)} %param.16), kind=kOutput, calls=%fused_computation.5 | convolution fusion | flops 1359446016 | bytes 9766912 | tf_op jit(solution)/shard_map/dot_general | solution.py:14
  29.6 0.6 copy-done.7
  30.2 0.6 dynamic-slice
  31.6 11.8 %all-reduce = f32[320]{0:T(512)S(1)} all-reduce(f32[320]{0:T(512)S(1)} %fusion.13), channel_id=3, replica_groups=mesh['kv'=8,'tp'=4] {'kv'}, use_global_device_ids=true, to_apply=%region_2.0.clone | all-reduce | flops 320 | bytes 2560
  43.5 44.5 %reduce-scatter.5.cloned.1.call-done = f32[40,4096]{1,0:T(8,128)} async-done(((f32[320,4096]{1,0:T(8,128)}), f32[40,4096]{1,0:T(8,128)}) %reduce-scatter.5.cloned.1.call-update) | async-done | bytes 655376 | tf_op jit(solution)/shard_map/reduce_scatter | solution.py:16
  87.9 1.2 broadcast_multiply_fusion.1
  89.4 15.0 %multiply_add_fusion = f32[40,8,128,128]{3,2,1,0:T(8,128)S(1)} fusion(f32[40,8,128,128]{3,2,1,0:T(8,128)} %param.15, f32[40,8,128]{2,1,0:T(8,128)S(1)} %bitcast.33, f32[40,8,128]{2,1,0:T(8,128)S(1)} %broadcast_subtract_fusion, f32[40,8,128]{2,1,0:T(8,128)S(1)} %bitcast.30), kind=kLoop, calls=%fused_computation | loop fusion | flops 15728640 | bytes 42434560 | tf_op jit(solution)/shard_map/add | solution.py:67
  104.5 17.9 %fusion.34 = f32[40,8,1,128]{3,2,1,0:T(1,128)S(1)} fusion(f32[40,8,128,1]{2,3,1,0:T(1,128)S(1)} %bitcast.31, f32[40,8,128,128]{3,2,1,0:T(8,128)S(1)} %multiply_add_fusion), kind=kOutput, calls=%fused_computation.53 | convolution fusion | flops 62914560 | bytes 21299200 | tf_op jit(solution)/shard_map/bhk,bhkv->bhv/dot_general | solution.py:68
  122.8 10.1 %all_gather.13 = bf16[320,1024]{1,0:T(8,128)(2,1)S(1)} all-gather(bf16[40,1024]{1,0:T(8,128)(2,1)S(1)} %fusion.21), channel_id=1, replica_groups=mesh['kv'=8,'tp'=4] {'kv'}, dimensions={0}, use_global_device_ids=true | all-gather | bytes 737280 | tf_op jit(solution)/shard_map/all_gather | solution.py:25
  132.9 1.4 fusion.35
  134.3 22.7 %reduce-scatter.7.cloned.1.call-done = f32[80,512]{1,0:T(8,128)} async-done(((f32[320,512]{1,0:T(8,128)}), f32[80,512]{1,0:T(8,128)}) %reduce-scatter.7.cloned.1.call-update) | async-done | bytes 163856 | tf_op jit(solution)/shard_map/reduce_scatter | solution.py:32
  157.0 0.9 add_convert_fusion.1
  157.9 14.9 %all_gather.14 = bf16[320,512]{1,0:T(8,128)(2,1)S(1)} all-gather(bf16[80,512]{1,0:T(8,128)(2,1)S(1)} %add_convert_fusion.1), channel_id=1, replica_groups=mesh['kv'=8,'tp'=4] {'tp'}, dimensions={0}, use_global_device_ids=true | all-gather | bytes 409600 | tf_op jit(solution)/shard_map/all_gather | solution.py:10
  172.9 7.1 %fusion = f32[320,5120]{1,0:T(8,128)} fusion(bf16[512,2560]{1,0:T(8,128)(2,1)} %param.26, bf16[512,2560]{1,0:T(8,128)(2,1)} %param.25, bf16[320,512]{1,0:T(8,128)(2,1)S(1)} %all_gather.14, f32[512]{0:T(512)S(1)} %copy-done.6), kind=kOutput, calls=%fused_computation.1 | convolution fusion | flops 1688698880 | bytes 12126208 | tf_op jit(solution)/shard_map/dot_general | solution.py:14
  180.1 0.2 fusion.15
  180.2 11.8 %all-reduce.1 = f32[320]{0:T(512)S(1)} all-reduce(f32[320]{0:T(512)S(1)} %fusion.15), channel_id=6, replica_groups=mesh['kv'=8,'tp'=4] {'kv'}, use_global_device_ids=true, to_apply=%region_7.8.clone | all-reduce | flops 320 | bytes 2560
  192.1 49.9 %reduce-scatter.9.cloned.1.call-done = f32[40,5120]{1,0:T(8,128)} async-done(((f32[320,5120]{1,0:T(8,128)}), f32[40,5120]{1,0:T(8,128)}) %reduce-scatter.9.cloned.1.call-update) | async-done | bytes 819216 | tf_op jit(solution)/shard_map/reduce_scatter | solution.py:16
  242.0 1.3 broadcast_multiply_fusion
  243.3 0.8 fusion.16
  244.1 25.9 %all-gather.2.cloned.1.call-done = bf16[320,2560]{1,0:T(8,128)(2,1)} async-done(((bf16[40,2560]{1,0:T(8,128)(2,1)}), bf16[320,2560]{1,0:T(8,128)(2,1)}) %all-gather.2.cloned.1.call-update) | async-done | bytes 1638416 | tf_op jit(solution)/shard_map/all_gather | solution.py:25
  270.1 3.3 %fusion.36 = f32[320,512]{1,0:T(8,128)} fusion(bf16[320,2560]{1,0:T(8,128)(2,1)} %all-gather.2.cloned.1.call-done, bf16[2560,512]{1,0:T(8,128)(2,1)S(1)} %copy-done), kind=kOutput, calls=%fused_computation.55 | convolution fusion | flops 838860800 | bytes 4915200 | tf_op jit(solution)/shard_map/dot_general | solution.py:24
  273.4 22.7 %reduce-scatter.11.cloned.1.call-done = f32[80,512]{1,0:T(8,128)} async-done(((f32[320,512]{1,0:T(8,128)}), f32[80,512]{1,0:T(8,128)}) %reduce-scatter.11.cloned.1.call-update) | async-done | bytes 163856 | tf_op jit(solution)/shard_map/reduce_scatter | solution.py:32
  296.1 1.6 add_convert_fusion
  (38 shorter events, 1.2 us)
Async XLA Ops:
  7.2 262.9 %copy-start = (bf16[2560,512]{1,0:T(8,128)(2,1)S(1)}, bf16[2560,512]{1,0:T(8,128)(2,1)}, u32[]{:S(2)}) copy-start(bf16[2560,512]{1,0:T(8,128)(2,1)} %param.27) | copy-start | bytes 7864324
  7.2 80.8 %reduce-scatter.5.cloned.1.call-start = ((), (), s32[]{:S(2)}) async-start(), calls=%async_computation.4 | async-start | bytes 5898240 | tf_op jit(solution)/shard_map/reduce_scatter | solution.py:16
  29.5 0.7 copy-start.7
  29.5 14.0 %copy-start.4 = (f32[1024]{0:T(1024)S(1)}, f32[1024]{0:T(1024)}, u32[]{:S(2)}) copy-start(f32[1024]{0:T(1024)} %param.21) | copy-start | bytes 12292
  29.5 127.5 %reduce-scatter.7.cloned.1.call-start = ((), (), s32[]{:S(2)}) async-start(), calls=%async_computation.5 | async-start | bytes 819200 | tf_op jit(solution)/shard_map/reduce_scatter | solution.py:32
  104.4 18.0 %copy-start.1 = (f32[40,8,128,128]{3,2,1,0:T(8,128)}, f32[40,8,128,128]{3,2,1,0:T(8,128)S(1)}, u32[]{:S(2)}) copy-start(f32[40,8,128,128]{3,2,1,0:T(8,128)S(1)} %multiply_add_fusion) | copy-start | bytes 62914564
  104.5 18.1 %copy-start.5 = (f32[128]{0:T(128)S(1)}, f32[128]{0:T(128)}, u32[]{:S(2)}) copy-start(f32[128]{0:T(128)} %param.22) | copy-start | bytes 1540
  104.5 28.4 %copy-start.2 = (bf16[1024,512]{1,0:T(8,128)(2,1)S(1)}, bf16[1024,512]{1,0:T(8,128)(2,1)}, u32[]{:S(2)}) copy-start(bf16[1024,512]{1,0:T(8,128)(2,1)} %param.23) | copy-start | bytes 3145732
  104.5 52.5 %copy-start.3 = (bf16[80,512]{1,0:T(8,128)(2,1)S(1)}, bf16[80,512]{1,0:T(8,128)(2,1)}, u32[]{:S(2)}) copy-start(bf16[80,512]{1,0:T(8,128)(2,1)} %param.14) | copy-start | bytes 245764
  122.4 50.4 %copy-start.6 = (f32[512]{0:T(512)S(1)}, f32[512]{0:T(512)}, u32[]{:S(2)}) copy-start(f32[512]{0:T(512)} %param.24) | copy-start | bytes 6148
  134.2 107.8 %reduce-scatter.9.cloned.1.call-start = ((), (), s32[]{:S(2)}) async-start(), calls=%async_computation.6 | async-start | bytes 7372800 | tf_op jit(solution)/shard_map/reduce_scatter | solution.py:16
  180.0 90.1 %all-gather.2.cloned.1.call-start = ((), (), s32[]{:S(2)}) async-start(), calls=%async_computation.7 | async-start | bytes 1843200 | tf_op jit(solution)/shard_map/all_gather | solution.py:25
  244.1 52.0 %reduce-scatter.11.cloned.1.call-start = ((), (), s32[]{:S(2)}) async-start(), calls=%async_computation.8 | async-start | bytes 819200 | tf_op jit(solution)/shard_map/reduce_scatter | solution.py:32
Sparse Core Ops, SparseCore 0:
  29.7 58.2 reduce-scatter.4
  134.4 22.5 reduce-scatter.6
  180.1 61.7 reduce-scatter.8
  244.2 25.8 all-gather.1
  273.5 22.5 reduce-scatter.10
where the time goes:
time: 305 us; the launch traced here: 304 us
  waiting for transfers between devices  166 us (54%)
  blocking collectives  64.9 us (21%)
  matrix products  35.8 us (12%)
  other arithmetic  21.7 us (7%)
  between operations  14.6 us (5%)
    reduce_scatter x2, waiting for transfers between devices, project_in(): lax.psum_scatter(product, 'kv', scatter_dimension=0, tiled=True)  94.3 us
    reduce_scatter x2, waiting for transfers between devices, sum_widths(): return lax.psum_scatter(terms, 'tp', scatter_dimension=0, tiled=True)  45.5 us
    all_gather x2, blocking collectives, project_in(): rows_all = lax.all_gather(shard_rows, 'tp', axis=0, tiled=True)  31.1 us
    all_gather x1, waiting for transfers between devices, project_back(): lax.all_gather(shard_rows, 'kv', axis=0, tiled=True)  25.9 us
    unnamed x2, blocking collectives  23.6 us
    dot_general x1, matrix products, body(): jnp.einsum('bhk,bhkv->bhv', query, new_state, precision=lax.Precision.HIG...  17.9 us
    add x1, other arithmetic, body(): forget[..., None] * state + (1.0 - forget)[..., None] * value[:, :, None, :]  15 us
    dot_general x2, matrix products, project_in(): product = jnp.dot(normed, weight_joined, preferred_element_type=jnp.float32)  13.2 us
  transfers between devices with their start and end apart: 5, of which 5 were waited for; matrix products, arithmetic and copies ran while one was open for 0% of the time, Pallas kernels for 0%

commit v1 on v0

v1 whole, which is shorter than its diff:
```python
import functools

import jax
import jax.numpy as jnp
from jax import lax
from jax.experimental import pallas as pl
from jax.experimental.pallas import tpu as pltpu
from jax.sharding import PartitionSpec as P

EPS = 1e-05
F32 = jnp.float32
BF16 = jnp.bfloat16
LANES = 128
MESH = pl.DeviceIdType.MESH
ANY = pl.BlockSpec(memory_space=pl.ANY)
VMEM = pl.BlockSpec(memory_space=pltpu.VMEM)


def remote(src, dst, send, recv, axis, peer):
    return pltpu.make_async_remote_copy(
        src_ref=src,
        dst_ref=dst,
        send_sem=send,
        recv_sem=recv,
        device_id={axis: peer},
        device_id_type=MESH,
    )


def greet(n_kv, n_tp):
    kv, tp = lax.axis_index("kv"), lax.axis_index("tp")
    barrier = pltpu.get_barrier_semaphore()
    for axis, me, n in (("kv", kv, n_kv), ("tp", tp, n_tp)):
        for off in range(1, n):
            pl.semaphore_signal(
                barrier,
                inc=1,
                device_id={axis: lax.rem(me + off, n)},
                device_id_type=MESH,
            )
    pl.semaphore_wait(barrier, n_kv + n_tp - 2)


def partner_of(me):
    return me + 1 - 2 * lax.rem(me, 2)


def exchange_start(src_at, dst, send, recv, axis, n):
    me = lax.axis_index(axis)
    copies = []
    for off in range(1, n):
        peer = lax.rem(me + off, n)
        copy = remote(src_at(peer), dst.at[me], send.at[off], recv.at[off], axis, peer)
        copy.start()
        copies.append(copy)
    return copies


def gather_kv(own, gathered, send, recv, fsend, frecv, n):
    me = lax.axis_index("kv")
    half = n // 2
    mine = me // 2
    parity = lax.rem(me, 2)
    partner = partner_of(me)
    first = []
    for off in range(1, half):
        peer = lax.rem(mine + off, half) * 2 + parity
        copy = remote(own, gathered.at[me], send.at[off], recv.at[off], "kv", peer)
        copy.start()
        first.append(copy)
    pair = remote(own, gathered.at[me], fsend.at[0], frecv.at[0], "kv", partner)
    pair.start()
    gathered[me] = own[...]
    second = [pair]
    for off in range(1, half):
        first[off - 1].wait_recv()
        source = lax.rem(mine + half - off, half) * 2 + parity
        copy = remote(
            gathered.at[source], gathered.at[source], fsend.at[off], frecv.at[off], "kv", partner
        )
        copy.start()
        second.append(copy)
    for copy in second:
        copy.wait_recv()
    return first + second


class Scatter:
    def __init__(self, refs, n):
        (self.out, self.pair_in, self.mid, self.rest_in, self.ps, self.pr, self.rs, self.rr) = refs
        self.n = n
        self.half = n // 2
        self.me = lax.axis_index("kv")
        self.mine = self.me // 2
        self.parity = lax.rem(self.me, 2)
        self.pairs = []
        self.rests = []

    def put(self, c, cols, block):
        rows = block.shape[0] // self.n
        for j in range(self.n):
            self.out[c, j % 2, j // 2, :, cols] = block[j * rows : (j + 1) * rows].astype(BF16)

    def send_pair(self, c):
        copy = remote(
            self.out.at[c, 1 - self.parity],
            self.pair_in.at[c],
            self.ps.at[c],
            self.pr.at[c],
            "kv",
            partner_of(self.me),
        )
        copy.start()
        self.pairs.append(copy)

    def pair_sum(self, c, j):
        return self.out[c, self.parity, j].astype(F32) + self.pair_in[c, j].astype(F32)

    def send_rest(self, c):
        self.pairs[c].wait_recv()
        copies = []
        for off in range(1, self.half):
            j = lax.rem(self.mine + off, self.half)
            self.mid[c, off] = self.pair_sum(c, j).astype(BF16)
            copy = remote(
                self.mid.at[c, off],
                self.rest_in.at[c, off],
                self.rs.at[c, off],
                self.rr.at[c, off],
                "kv",
                j * 2 + self.parity,
            )
            copy.start()
            copies.append(copy)
        self.rests.append(copies)

    def total(self, c):
        for copy in self.rests[c]:
            copy.wait_recv()
        total = self.pair_sum(c, self.mine)
        for off in range(1, self.half):
            total = total + self.rest_in[c, off].astype(F32)
        return total

    def close(self):
        for copy in self.pairs:
            copy.wait_send()
        for copies in self.rests:
            for copy in copies:
                copy.wait_send()


def scatter_scratch(chunks, n, rows, cols):
    half = n // 2
    return [
        pltpu.VMEM((chunks, 2, half, rows, cols), BF16),
        pltpu.VMEM((chunks, half, rows, cols), BF16),
        pltpu.VMEM((chunks, half, rows, cols), BF16),
        pltpu.VMEM((chunks, half, rows, cols), BF16),
        pltpu.SemaphoreType.DMA((chunks,)),
        pltpu.SemaphoreType.DMA((chunks,)),
        pltpu.SemaphoreType.DMA((chunks, half)),
        pltpu.SemaphoreType.DMA((chunks, half)),
    ]


def squares_scratch(n, rows):
    return [
        pltpu.VMEM((n, rows, LANES), F32),
        pltpu.VMEM((n, rows, LANES), F32),
        pltpu.SemaphoreType.DMA((n,)),
        pltpu.SemaphoreType.DMA((n,)),
    ]


def squares_start(values, refs, n):
    out, into, send, recv = refs
    totals = jnp.sum(values * values, axis=1, keepdims=True)
    totals = jnp.broadcast_to(totals, (values.shape[0], LANES))
    out[...] = totals.reshape(out.shape)
    return exchange_start(lambda peer: out.at[peer], into, send, recv, "kv", n)


def squares_factor(copies, refs, n, width):
    out, into, _, _ = refs
    me = lax.axis_index("kv")
    for copy in copies:
        copy.wait_recv()
    total = out[me]
    for off in range(1, n):
        total = total + into[lax.rem(me + off, n)]
    return lax.rsqrt(total[:, :1] / width + EPS)


def tile_of(cols):
    return 512 if cols % 512 == 0 else cols


def mixer_in(n_kv, n_tp, width, tokens, gain, wq, wf, wv, wg, sums, rows_all, weights, *rest):
    scatter_refs, square_refs = rest[:8], rest[8:12]
    load_sem, t_send, t_recv = rest[12:]
    tp = lax.axis_index("tp")
    loads = [
        pltpu.make_async_copy(w, weights.at[i], load_sem.at[i])
        for i, w in enumerate((wq, wf, wv, wg))
    ]
    for load in loads:
        load.start()
    greet(n_kv, n_tp)
    copies = exchange_start(lambda peer: tokens, rows_all, t_send, t_recv, "tp", n_tp)
    rows_all[tp] = tokens[...]
    for copy in copies:
        copy.wait_recv()
    batch = n_tp * tokens.shape[0]
    values = rows_all[...].astype(F32).reshape(batch, tokens.shape[1])
    normed = (values * gain[...]).astype(BF16)
    scatter = Scatter(scatter_refs, n_kv)
    cols = weights.shape[2]
    tile = tile_of(cols)
    squares = None
    for c in range(4):
        loads[c].wait()
        for at in range(0, cols, tile):
            part = pl.ds(at, tile)
            scatter.put(
                c, part, jnp.dot(normed, weights[c, :, part], preferred_element_type=F32)
            )
        scatter.send_pair(c)
        if c > 0:
            scatter.send_rest(c - 1)
        if c == 0:
            squares = squares_start(values, square_refs, n_kv)
    scatter.send_rest(3)
    factor = squares_factor(squares, square_refs, n_kv, width)
    for c in range(4):
        sums[:, c * cols : (c + 1) * cols] = scatter.total(c) * factor
    for copy in copies + squares:
        copy.wait_send()
    scatter.close()


def state_step(q_pre, f_pre, v_pre, g_pre, bound, head_gain, state, new_state, gated, read):
    rows = q_pre.shape[0]
    size = state.shape[-1]
    low = bound[...]
    query = jax.nn.silu(q_pre[...]) * size ** (-0.5)
    forget = low + (1.0 - low) * jax.nn.sigmoid(f_pre[...])
    query_t = query.T
    forget_t = forget.T
    value = v_pre[...]
    for b in range(rows):
        v = value[b : b + 1, :]
        new = v + forget_t[:, b : b + 1] * (state[b, 0] - v)
        new_state[b, 0] = new
        read[b : b + 1, :] = jnp.sum(query_t[:, b : b + 1] * new, axis=0, keepdims=True)
    out = read[...]
    out = out * lax.rsqrt(jnp.mean(out * out, axis=1, keepdims=True) + EPS) * head_gain[...]
    gated[...] = (out * jax.nn.silu(g_pre[...])).astype(BF16)


def rest_of_layer(
    n_kv, n_tp, width, chunks, tokens, gated, gain, w_out, w_gate, w_up, w_down, out, *refs
):
    (v_out, v_ffn, v_down, g_all, h_own, h_all, t_acc, t_send_buf, t_recv_buf, r_own, r_all) = refs[:11]
    scatter_refs, square_refs = refs[11:19], refs[19:23]
    (load_sem, gs, gr, gfs, gfr, hs, hr, hfs, hfr, ts, tr) = refs[23:]
    tp = lax.axis_index("tp")
    loads = [
        pltpu.make_async_copy(w_out, v_out, load_sem.at[0]),
        pltpu.make_async_copy(w_gate, v_ffn.at[0], load_sem.at[1]),
        pltpu.make_async_copy(w_up, v_ffn.at[1], load_sem.at[2]),
        pltpu.make_async_copy(w_down, v_down, load_sem.at[3]),
    ]
    for load in loads:
        load.start()
    greet(n_kv, n_tp)
    done = []
    rows_tp = tokens.shape[0]

    def sum_tp(k, left, right):
        batch = n_tp * rows_tp
        values = left[...].astype(F32).reshape(batch, left.shape[2]).astype(BF16)
        product = jnp.dot(values, right[...], preferred_element_type=F32)
        product = product.reshape(n_tp, rows_tp, product.shape[1])
        t_acc[...] = product
        t_send_buf[k] = product.astype(BF16)
        copies = exchange_start(
            lambda peer: t_send_buf.at[k, peer], t_recv_buf.at[k], ts.at[k], tr.at[k], "tp", n_tp
        )
        total = t_acc[tp]
        for off in range(1, n_tp):
            copies[off - 1].wait_recv()
            total = total + t_recv_buf[k, lax.rem(tp + n_tp - off, n_tp)].astype(F32)
        done.extend(copies)
        return total

    done.extend(gather_kv(gated, g_all, gs, gr, gfs, gfr, n_kv))
    loads[0].wait()
    attended = sum_tp(0, g_all, v_out)
    r_own[...] = (tokens[...].astype(F32) + attended).astype(BF16)
    copies = exchange_start(lambda peer: r_own, r_all, ts.at[2], tr.at[2], "tp", n_tp)
    r_all[tp] = r_own[...]
    for copy in copies:
        copy.wait_recv()
    done.extend(copies)
    values = r_all[...].astype(F32).reshape(n_tp * rows_tp, tokens.shape[1])
    normed = (values * gain[...]).astype(BF16)
    scatter = Scatter(scatter_refs, n_kv)
    cols = v_ffn.shape[2]
    step = cols // chunks
    tile = next(t for t in (640, 512, 256, 128) if step % t == 0)
    order = [(w, h) for h in range(chunks) for w in range(2)]
    loads[1].wait()
    loads[2].wait()
    squares = None
    for c, (w, h) in enumerate(order):
        for at in range(0, step, tile):
            product = jnp.dot(
                normed, v_ffn[w, :, pl.ds(h * step + at, tile)], preferred_element_type=F32
            )
            scatter.put(c, pl.ds(at, tile), product)
        scatter.send_pair(c)
        if c > 0:
            scatter.send_rest(c - 1)
        if c == 0:
            squares = squares_start(values, square_refs, n_kv)
    scatter.send_rest(2 * chunks - 1)
    factor = squares_factor(squares, square_refs, n_kv, width)
    done.extend(squares)
    for h in range(chunks):
        gate = scatter.total(2 * h) * factor
        up = scatter.total(2 * h + 1) * factor
        h_own[:, h * step : (h + 1) * step] = (jax.nn.silu(gate) * up).astype(BF16)
    done.extend(gather_kv(h_own, h_all, hs, hr, hfs, hfr, n_kv))
    loads[3].wait()
    down = sum_tp(1, h_all, v_down)
    out[...] = (r_own[...].astype(F32) + down).astype(BF16)
    for copy in done:
        copy.wait_send()
    scatter.close()


def body(
    n_kv,
    n_tp,
    tokens,
    state,
    mix_gain,
    q_weight,
    forget_weight,
    input_weight,
    gate_weight,
    lower_bound,
    head_gain,
    out_weight,
    ffn_gain,
    ffn_gate,
    ffn_up,
    ffn_down,
):
    rows_tp, feats = tokens.shape
    width = feats * n_kv
    rows_kv, heads, size = state.shape[:3]
    cols = q_weight.shape[1]
    ff = ffn_gate.shape[1]
    dma = pltpu.SemaphoreType.DMA
    sums = pl.pallas_call(
        functools.partial(mixer_in, n_kv, n_tp, width),
        out_shape=jax.ShapeDtypeStruct((rows_kv, 4 * cols), F32),
        in_specs=[VMEM, VMEM, ANY, ANY, ANY, ANY],
        out_specs=VMEM,
        scratch_shapes=[
            pltpu.VMEM((n_tp, rows_tp, feats), BF16),
            pltpu.VMEM((4, feats, cols), BF16),
            *scatter_scratch(4, n_kv, rows_kv, cols),
            *squares_scratch(n_kv, rows_kv),
            dma((4,)),
            dma((n_tp,)),
            dma((n_tp,)),
        ],
        compiler_params=pltpu.CompilerParams(collective_id=0, has_side_effects=True),
        name="mixer_in",
    )(tokens, mix_gain[None, :], q_weight, forget_weight, input_weight, gate_weight)

    def part(i):
        return pl.BlockSpec((rows_kv, size), lambda h: (0, i * heads + h))

    state_block = pl.BlockSpec((rows_kv, 1, size, size), lambda h: (0, h, 0, 0))
    new_state, gated = pl.pallas_call(
        state_step,
        out_shape=(
            jax.ShapeDtypeStruct(state.shape, F32),
            jax.ShapeDtypeStruct((rows_kv, cols), BF16),
        ),
        grid=(heads,),
        in_specs=[
            part(0),
            part(1),
            part(2),
            part(3),
            pl.BlockSpec((1, size), lambda h: (0, h)),
            pl.BlockSpec((1, size), lambda h: (0, 0)),
            state_block,
        ],
        out_specs=(state_block, pl.BlockSpec((rows_kv, size), lambda h: (0, h))),
        scratch_shapes=[pltpu.VMEM((rows_kv, size), F32)],
        compiler_params=pltpu.CompilerParams(dimension_semantics=("arbitrary",)),
        name="state_step",
    )(sums, sums, sums, sums, lower_bound[None, :], head_gain[None, :], state)

    half = n_kv // 2
    chunks = 2 if ff % (2 * LANES) == 0 else 1
    layer_out = pl.pallas_call(
        functools.partial(rest_of_layer, n_kv, n_tp, width, chunks),
        out_shape=jax.ShapeDtypeStruct(tokens.shape, BF16),
        in_specs=[VMEM, VMEM, VMEM, ANY, ANY, ANY, ANY],
        out_specs=VMEM,
        scratch_shapes=[
            pltpu.VMEM((cols, feats), BF16),
            pltpu.VMEM((2, feats, ff), BF16),
            pltpu.VMEM((ff, feats), BF16),
            pltpu.VMEM((n_kv, rows_kv, cols), BF16),
            pltpu.VMEM((rows_kv, ff), BF16),
            pltpu.VMEM((n_kv, rows_kv, ff), BF16),
            pltpu.VMEM((n_tp, rows_tp, feats), F32),
            pltpu.VMEM((2, n_tp, rows_tp, feats), BF16),
            pltpu.VMEM((2, n_tp, rows_tp, feats), BF16),
            pltpu.VMEM((rows_tp, feats), BF16),
            pltpu.VMEM((n_tp, rows_tp, feats), BF16),
            *scatter_scratch(2 * chunks, n_kv, rows_kv, ff // chunks),
            *squares_scratch(n_kv, rows_kv),
            dma((4,)),
            *[dma((half,)) for _ in range(8)],
            dma((3, n_tp)),
            dma((3, n_tp)),
        ],
        compiler_params=pltpu.CompilerParams(collective_id=1, has_side_effects=True),
        name="rest_of_layer",
    )(tokens, gated, ffn_gain[None, :], out_weight, ffn_gate, ffn_up, ffn_down)
    return (layer_out, new_state)


def solution(mesh):
    in_specs = (
        P("tp", "kv"),
        P("kv", "tp", None, None),
        P("kv"),
        P("kv", "tp"),
        P("kv", "tp"),
        P("kv", "tp"),
        P("kv", "tp"),
        P("tp"),
        P(),
        P("tp", "kv"),
        P("kv"),
        P("kv", "tp"),
        P("kv", "tp"),
        P("tp", "kv"),
    )
    out_specs = (P("tp", "kv"), P("kv", "tp", None, None))
    step = functools.partial(body, mesh.shape["kv"], mesh.shape["tp"])
    return jax.shard_map(step, mesh=mesh, in_specs=in_specs, out_specs=out_specs, check_vma=False)
```

time: 305 us -> 129 us (0.42)
  waiting for transfers between devices: 166 us -> 0 us
  Pallas kernels: 0 us -> 127 us
  blocking collectives: 64.9 us -> 0 us
  matrix products: 35.8 us -> 0 us
  other arithmetic: 21.7 us -> 0 us
  between operations: 14.6 us -> 0.65 us
    reduce_scatter x4 -> x0, waiting for transfers between devices: 140 us -> none  [the longest x2 94.3 us: project_in(): lax.psum_scatter(product, 'kv', scatter_dimension=0, tiled=True)]
    pallas_call x0 -> x3, Pallas kernels: none -> 127 us  [the longest x1 72.3 us: body(): pl.pallas_call(functools.partial(rest_of_layer, n_kv, n_tp, width, chunks...]
    all_gather x3 -> x0, blocking collectives: 41.2 us -> none  [the longest x2 31.1 us: project_in(): rows_all = lax.all_gather(shard_rows, 'tp', axis=0, tiled=True)]
    dot_general x5 -> x0, matrix products: 35.8 us -> none  [the longest x1 17.9 us: body(): jnp.einsum('bhk,bhkv->bhv', query, new_state, precision=lax.Precision.HIG...]
    all_gather x1 -> x0, waiting for transfers between devices: 25.9 us -> none  [project_back(): lax.all_gather(shard_rows, 'kv', axis=0, tiled=True)]
    unnamed x2 -> x0, blocking collectives: 23.6 us -> none
    add x1 -> x0, other arithmetic: 15 us -> none  [body(): forget[..., None] * state + (1.0 - forget)[..., None] * value[:, :, None, :]]
    convert_element_type x4 -> x0, other arithmetic: 3.37 us -> none  [the longest x1 1.57 us: body(): (own_rows.astype(jnp.float32) + sum_widths(project_back(hidden, ffn_down)...]
  transfers between devices with their start and end apart: 5 -> 0, of which waited for: 5 -> 0; matrix products, arithmetic and copies ran while one was open for 0% -> 0% of each run, Pallas kernels for 0% -> 0%
where the time goes in v1:
time: 129 us
  Pallas kernels  127 us (98%)
  local copies, waits for them, and re-layouts  1.53 us (1%)
    pallas_call x1, Pallas kernels, body(): pl.pallas_call(functools.partial(rest_of_layer, n_kv, n_tp, width, chunks...  72.3 us
    pallas_call x1, Pallas kernels, body(): pl.pallas_call(functools.partial(mixer_in, n_kv, n_tp, width), out_shape=...  33.6 us
    pallas_call x1, Pallas kernels, body(): pl.pallas_call(state_step, out_shape=(jax.ShapeDtypeStruct(state.shape, F...  20.8 us

profile of v1, /device:TPU:0, one launch (start us, length us, event | category | flops | bytes accessed | tf_op | source)
XLA Modules:
  0.0 128.9 jit_solution(17346049646217911308)
XLA Ops:
  0.6 33.6 %mixer_in.1.q_pre.f_pre.v_pre.g_pre = f32[40,4096]{1,0:T(8,128)} custom-call(bf16[80,512]{1,0:T(8,128)(2,1)} %tokens.3, f32[1,512]{1,0:T(1,128)} %bitcast.5, bf16[512,1024]{1,0:T(8,128)(2,1)} %wq.1, bf16[512,1024]{1,0:T(8,128)(2,1)} %wf.1, bf16[512,1024]{1,0:T(8,128)(2,1)} %wv.1, bf16[512,1024]{1,0:T(8,128)(2,1)} %wg.1), custom_call_target="tpu_custom_call" | custom-call | tf_op jit(solution)/shard_map/mixer_in/pallas_call | solution.py:367
  34.2 20.8 %state_step.1 = (f32[40,8,128,128]{3,2,1,0:T(8,128)}, bf16[40,1024]{1,0:T(8,128)(2,1)}) custom-call(f32[40,4096]{1,0:T(8,128)} %mixer_in.1.q_pre.f_pre.v_pre.g_pre, f32[40,4096]{1,0:T(8,128)} %mixer_in.1.q_pre.f_pre.v_pre.g_pre, f32[40,4096]{1,0:T(8,128)} %mixer_in.1.q_pre.f_pre.v_pre.g_pre, f32[40,4096]{1,0:T(8,128)} %mixer_in.1.q_pre.f_pre.v_pre.g_pre, ...), custom_call_target="tpu_custom_call" | custom-call | tf_op jit(solution)/shard_map/state_step/pallas_call | solution.py:389
  55.0 72.3 %rest_of_layer.1 = bf16[80,512]{1,0:T(8,128)(2,1)} custom-call(bf16[80,512]{1,0:T(8,128)(2,1)} %tokens.3, bf16[40,1024]{1,0:T(8,128)(2,1)} %get-tuple-element.4.gated, f32[1,512]{1,0:T(1,128)} %bitcast.6, bf16[1024,512]{1,0:T(8,128)(2,1)} %w_out.1, bf16[512,2560]{1,0:T(8,128)(2,1)} %w_gate.1, bf16[512,2560]{1,0:T(8,128)(2,1)} %w_up.1, bf16[2560,512]{1,0:T(8,128)(2,1)} %w_down.1), custom_call_target="tpu_custom_call" | custom-call | tf_op jit(solution)/shard_map/rest_of_layer/pallas_call | solution.py:413
  127.3 1.5 %copy.17 = bf16[80,512]{1,0:T(8,128)(2,1)} copy(bf16[80,512]{1,0:T(8,128)(2,1)} %rest_of_layer.1) | data formatting | bytes 163840

commit v2 on v1

--- a/solution.py
+++ b/solution.py
@@ -11,8 +11,9 @@
 F32 = jnp.float32
 BF16 = jnp.bfloat16
 LANES = 128
+MIB = 1 << 20
 MESH = pl.DeviceIdType.MESH
-ANY = pl.BlockSpec(memory_space=pl.ANY)
+HBM = pl.BlockSpec(memory_space=pltpu.HBM)
 VMEM = pl.BlockSpec(memory_space=pltpu.VMEM)
 
 
@@ -367,7 +368,7 @@
     sums = pl.pallas_call(
         functools.partial(mixer_in, n_kv, n_tp, width),
         out_shape=jax.ShapeDtypeStruct((rows_kv, 4 * cols), F32),
-        in_specs=[VMEM, VMEM, ANY, ANY, ANY, ANY],
+        in_specs=[VMEM, VMEM, HBM, HBM, HBM, HBM],
         out_specs=VMEM,
         scratch_shapes=[
             pltpu.VMEM((n_tp, rows_tp, feats), BF16),
@@ -378,7 +379,14 @@
             dma((n_tp,)),
             dma((n_tp,)),
         ],
-        compiler_params=pltpu.CompilerParams(collective_id=0, has_side_effects=True),
+        compiler_params=pltpu.CompilerParams(
+            collective_id=0, has_side_effects=True, vmem_limit_bytes=min(60 * MIB, 67043328 - state.size * 4 - MIB)
+        ),
+        cost_estimate=pl.CostEstimate(
+            flops=32 * n_tp * rows_tp * feats * 4 * cols,
+            bytes_accessed=16 * feats * 4 * cols,
+            transcendentals=0,
+        ),
         name="mixer_in",
     )(tokens, mix_gain[None, :], q_weight, forget_weight, input_weight, gate_weight)
 
@@ -404,7 +412,12 @@
         ],
         out_specs=(state_block, pl.BlockSpec((rows_kv, size), lambda h: (0, h))),
         scratch_shapes=[pltpu.VMEM((rows_kv, size), F32)],
-        compiler_params=pltpu.CompilerParams(dimension_semantics=("arbitrary",)),
+        compiler_params=pltpu.CompilerParams(dimension_semantics=("arbitrary",), vmem_limit_bytes=16 * MIB),
+        cost_estimate=pl.CostEstimate(
+            flops=6 * rows_kv * heads * size * size,
+            bytes_accessed=8 * rows_kv * heads * size * size,
+            transcendentals=0,
+        ),
         name="state_step",
     )(sums, sums, sums, sums, lower_bound[None, :], head_gain[None, :], state)
 
@@ -413,7 +426,7 @@
     layer_out = pl.pallas_call(
         functools.partial(rest_of_layer, n_kv, n_tp, width, chunks),
         out_shape=jax.ShapeDtypeStruct(tokens.shape, BF16),
-        in_specs=[VMEM, VMEM, VMEM, ANY, ANY, ANY, ANY],
+        in_specs=[VMEM, VMEM, VMEM, HBM, HBM, HBM, HBM],
         out_specs=VMEM,
         scratch_shapes=[
             pltpu.VMEM((cols, feats), BF16),

time: 129 us -> 138 us (1.070)
  local copies, waits for them, and re-layouts: 1.53 us -> 15.6 us
  Pallas kernels: 127 us -> 121 us
    unnamed x1 -> x21, local copies, waits for them, and re-layouts: 1.53 us -> 15.6 us
    pallas_call x1, Pallas kernels: 20.8 us -> 16.5 us  [body(): pl.pallas_call(state_step, out_shape=(jax.ShapeDtypeStruct(state.shape, F...]
where the time goes in v2:
time: 138 us; the launch traced here: 137 us
  Pallas kernels  121 us (88%)
  local copies, waits for them, and re-layouts  15.6 us (11%)
    pallas_call x1, Pallas kernels, body(): pl.pallas_call(functools.partial(rest_of_layer, n_kv, n_tp, width, chunks...  72.3 us
    pallas_call x1, Pallas kernels, body(): pl.pallas_call(functools.partial(mixer_in, n_kv, n_tp, width), out_shape=...  32.2 us
    pallas_call x1, Pallas kernels, body(): pl.pallas_call(state_step, out_shape=(jax.ShapeDtypeStruct(state.shape, F...  16.5 us
    unnamed x21, local copies, waits for them, and re-layouts  15.6 us

profile of v2, /device:TPU:0, one launch (start us, length us, event | category | flops | bytes accessed | tf_op | source)
XLA Modules:
  0.0 137.3 jit_solution(1200877420247838731)
XLA Ops:
  0.6 0.0 copy-start.1
  0.6 0.9 copy-done.1
  1.5 0.0 copy-start.5
  1.5 1.2 copy-done.5
  2.7 0.0 copy-start.6
  2.8 1.2 copy-done.6
  4.0 0.0 copy-start.7
  4.0 1.2 copy-done.7
  5.2 0.0 copy-start.8
  5.2 1.2 copy-done.8
  6.4 0.0 copy-start.9
  6.4 0.7 copy-done.9
  7.1 0.0 copy-start.3
  7.1 0.0 copy-start.4
  7.1 32.2 %mixer_in.1.q_pre.f_pre.v_pre.g_pre = f32[40,4096]{1,0:T(8,128)S(1)} custom-call(bf16[80,512]{1,0:T(8,128)(2,1)S(1)} %copy-done.1, f32[1,512]{1,0:T(1,128)S(1)} %bitcast.6, bf16[512,1024]{1,0:T(8,128)(2,1)S(1)} %copy-done.5, bf16[512,1024]{1,0:T(8,128)(2,1)S(1)} %copy-done.6, bf16[512,1024]{1,0:T(8,128)(2,1)S(1)} %copy-done.7, bf16[512,1024]{1,0:T(8,128)(2,1)S(1)} %copy-done.8), custom_call_target="tpu_custom_call" | custom-call | flops 21474836480 | bytes 33554432 | tf_op jit(solution)/shard_map/mixer_in/pallas_call | solution.py:368
  39.3 0.0 copy-done.3
  39.3 0.0 copy-done.4
  39.4 0.0 copy-start
  39.4 7.0 %copy-done = f32[40,8,128,128]{3,2,1,0:T(8,128)S(1)} copy-done((f32[40,8,128,128]{3,2,1,0:T(8,128)S(1)}, f32[40,8,128,128]{3,2,1,0:T(8,128)}, u32[]{:S(2)}) %copy-start) | copy-done | bytes 20971544
  46.3 16.5 %state_step.1 = (f32[40,8,128,128]{3,2,1,0:T(8,128)}, bf16[40,1024]{1,0:T(8,128)(2,1)S(1)}) custom-call(f32[40,4096]{1,0:T(8,128)S(1)} %mixer_in.1.q_pre.f_pre.v_pre.g_pre, f32[40,4096]{1,0:T(8,128)S(1)} %mixer_in.1.q_pre.f_pre.v_pre.g_pre, f32[40,4096]{1,0:T(8,128)S(1)} %mixer_in.1.q_pre.f_pre.v_pre.g_pre, f32[40,4096]{1,0:T(8,128)S(1)} %mixer_in.1.q_pre.f_pre.v_pre.g_pre, ...), custom_call_target="tpu_custom_call" | custom-call | flops 31457280 | bytes 41943040 | tf_op jit(solution)/shard_map/state_step/pallas_call | solution.py:397
  62.8 0.0 copy-start.2
  62.8 0.6 copy-done.2
  63.5 72.3 %rest_of_layer.1 = bf16[80,512]{1,0:T(8,128)(2,1)} custom-call(bf16[80,512]{1,0:T(8,128)(2,1)} %tokens.3, bf16[40,1024]{1,0:T(8,128)(2,1)} %copy-done.2, f32[1,512]{1,0:T(1,128)} %bitcast.7, bf16[1024,512]{1,0:T(8,128)(2,1)} %w_out.1, bf16[512,2560]{1,0:T(8,128)(2,1)} %w_gate.1, bf16[512,2560]{1,0:T(8,128)(2,1)} %w_up.1, bf16[2560,512]{1,0:T(8,128)(2,1)} %w_down.1), custom_call_target="tpu_custom_call" | custom-call | tf_op jit(solution)/shard_map/rest_of_layer/pallas_call | solution.py:426
  135.8 1.5 %copy.17 = bf16[80,512]{1,0:T(8,128)(2,1)} copy(bf16[80,512]{1,0:T(8,128)(2,1)} %rest_of_layer.1) | data formatting | bytes 163840
Async XLA Ops:
  0.6 0.9 copy-start.1
  1.5 1.2 copy-start.5
  2.7 1.2 copy-start.6
  4.0 1.2 copy-start.7
  5.2 1.2 copy-start.8
  6.4 0.7 copy-start.9
  7.1 32.2 %copy-start.3 = (f32[1024]{0:T(1024)S(1)}, f32[1024]{0:T(1024)}, u32[]{:S(2)}) copy-start(f32[1024]{0:T(1024)} %param.21) | copy-start | bytes 12292
  7.1 32.2 %copy-start.4 = (f32[128]{0:T(128)S(1)}, f32[128]{0:T(128)}, u32[]{:S(2)}) copy-start(f32[128]{0:T(128)} %param.22) | copy-start | bytes 1540
  39.4 7.0 %copy-start = (f32[40,8,128,128]{3,2,1,0:T(8,128)S(1)}, f32[40,8,128,128]{3,2,1,0:T(8,128)}, u32[]{:S(2)}) copy-start(f32[40,8,128,128]{3,2,1,0:T(8,128)} %state.1) | copy-start | bytes 62914564
  62.8 0.6 copy-start.2
